TPU v7x, 32 devices: a whole 2x2x4 slice. The times are simulated.
32 devices in a mesh: grp: 2 (over y), dp: 2 (over x), kv: 4 (over z), tp: 2 (over core).
Axes of the slice: x: 2, y: 2, z: 4, core: 2. Of those that a mesh axis runs over, the one named last changes fastest.
Arguments:
- residual_input: bfloat16 [128, 4096], P(('grp', 'dp', 'tp'), 'kv'), parts along dimension 0, may hold values from -6 to 6
- incoming_state: float32 [128, 16, 64, 128], P(('grp', 'kv'), ('dp', 'tp')), parts along dimension 0, may hold values from -4 to 4
- extra_log_decay: float32 [128, 1024], P(('grp', 'kv'), ('dp', 'tp')), parts along dimension 0, may hold values from -0.7 to 0
- leading_norm_gain: float32 [4096], P('kv'), may hold values from 0.1 to 1.9
- leading_gate_weight: bfloat16 [4096, 11264], P('kv', ('dp', 'tp')), may hold values from -0.09375 to 0.09375
- leading_up_weight: bfloat16 [4096, 11264], P('kv', ('dp', 'tp')), may hold values from -0.09375 to 0.09375
- leading_down_weight: bfloat16 [11264, 4096], P(('dp', 'tp'), 'kv'), may hold values from -0.0546875 to 0.0546875
- attention_norm_gain: float32 [4096], P('kv'), may hold values from 0.1 to 1.9
- query_projector: bfloat16 [4096, 1024], P('kv', ('dp', 'tp')), may hold values from -0.09375 to 0.09375
- key_projector: bfloat16 [4096, 1024], P('kv', ('dp', 'tp')), may hold values from -0.09375 to 0.09375
- value_projector: bfloat16 [4096, 2048], P('kv', ('dp', 'tp')), may hold values from -0.09375 to 0.09375
- output_gate_weight: bfloat16 [4096, 2048], P('kv', ('dp', 'tp')), may hold values from -0.09375 to 0.09375
- forget_weight: bfloat16 [4096, 1024], P('kv', ('dp', 'tp')), may hold values from -0.75 to 0.75
- head_norm_gain: float32 [128], replicated, may hold values from 0.1 to 1.9
- output_projector: bfloat16 [2048, 4096], P(('dp', 'tp'), 'kv'), may hold values from -0.125 to 0.125
- trailing_norm_gain: float32 [4096], P('kv'), may hold values from 0.1 to 1.9
- trailing_gate_weight: bfloat16 [4096, 11264], P('kv', ('dp', 'tp')), may hold values from -0.09375 to 0.09375
- trailing_up_weight: bfloat16 [4096, 11264], P('kv', ('dp', 'tp')), may hold values from -0.09375 to 0.09375
- trailing_down_weight: bfloat16 [11264, 4096], P(('dp', 'tp'), 'kv'), may hold values from -0.0546875 to 0.0546875
Outputs:
- result: bfloat16 [128, 4096], P(('grp', 'dp', 'tp'), 'kv'), parts along dimension 0
- new_state: float32 [128, 16, 64, 128], P(('grp', 'kv'), ('dp', 'tp')), parts along dimension 0
There are 2 independent parts, one for each index of `grp`. A program takes and returns all parts, laid end to end along the dimension named above; an argument that names none is the same for every part. Nothing has to cross between parts.
All inputs are finite; a program needn't handle non-finite values.
Results may differ from a plain program's by a relative error of at most 0.0095.
Values may be sent and summed in bfloat16 or wider, within the bound.
A program may use at most 128 MiB of HBM per device.

v0:
```python
import jax
import jax.numpy as jnp
from jax import lax
from jax.sharding import PartitionSpec as P

D = 4096
KEY_CHANNELS = 64
VALUE_DIM = 128
epsilon = 1e-06


def batch_rows(row_block):
    return lax.all_gather(row_block, ("dp", "tp"), axis=0, tiled=True)


def channel_mixer(row_block, norm_gain, gate_matrix, up_matrix, down_matrix):
    gathered = batch_rows(row_block)
    widened = gathered.astype(jnp.float32)
    squares = jnp.sum(widened * widened, axis=1)
    scaled = (widened * norm_gain).astype(jnp.bfloat16)
    gate_part = jnp.dot(scaled, gate_matrix, preferred_element_type=jnp.float32)
    up_part = jnp.dot(scaled, up_matrix, preferred_element_type=jnp.float32)
    gate_sum, up_sum, row_total = (
        lax.psum_scatter(gate_part, "kv", scatter_dimension=0, tiled=True),
        lax.psum_scatter(up_part, "kv", scatter_dimension=0, tiled=True),
        lax.psum_scatter(squares, "kv", scatter_dimension=0, tiled=True),
    )
    decay_factor = lax.rsqrt(row_total / D + epsilon)[:, None]
    hidden_share = (jax.nn.silu(decay_factor * gate_sum) * (decay_factor * up_sum)).astype(
        jnp.bfloat16
    )
    hidden = lax.all_gather(hidden_share, "kv", axis=0, tiled=True)
    return lax.psum_scatter(
        jnp.dot(hidden, down_matrix, preferred_element_type=jnp.float32),
        ("dp", "tp"),
        scatter_dimension=0,
        tiled=True,
    )


def per_device(
    residual_input,
    incoming_state,
    extra_log_decay,
    leading_norm_gain,
    leading_gate_weight,
    leading_up_weight,
    leading_down_weight,
    attention_norm_gain,
    query_projector,
    key_projector,
    value_projector,
    output_gate_weight,
    forget_weight,
    head_norm_gain,
    output_projector,
    trailing_norm_gain,
    trailing_gate_weight,
    trailing_up_weight,
    trailing_down_weight,
):
    after_first = (
        residual_input.astype(jnp.float32)
        + 0.5
        * channel_mixer(
            residual_input,
            leading_norm_gain,
            leading_gate_weight,
            leading_up_weight,
            leading_down_weight,
        )
    ).astype(jnp.bfloat16)
    gathered = batch_rows(after_first)
    widened = gathered.astype(jnp.float32)
    squares = jnp.sum(widened * widened, axis=1)
    scaled = (widened * attention_norm_gain).astype(jnp.bfloat16)
    query_part = jnp.dot(scaled, query_projector, preferred_element_type=jnp.float32)
    key_part = jnp.dot(scaled, key_projector, preferred_element_type=jnp.float32)
    value_part = jnp.dot(scaled, value_projector, preferred_element_type=jnp.float32)
    gate_part = jnp.dot(scaled, output_gate_weight, preferred_element_type=jnp.float32)
    decay_part = jnp.dot(scaled, forget_weight, preferred_element_type=jnp.float32)
    query_sum, key_sum, value_sum, gate_sum, decay_total, row_total = (
        lax.psum_scatter(query_part, "kv", scatter_dimension=0, tiled=True),
        lax.psum_scatter(key_part, "kv", scatter_dimension=0, tiled=True),
        lax.psum_scatter(value_part, "kv", scatter_dimension=0, tiled=True),
        lax.psum_scatter(gate_part, "kv", scatter_dimension=0, tiled=True),
        lax.psum_scatter(decay_part, "kv", scatter_dimension=0, tiled=True),
        lax.psum_scatter(squares, "kv", scatter_dimension=0, tiled=True),
    )
    decay_factor = lax.rsqrt(row_total / D + epsilon)[:, None]
    row_count = query_sum.shape[0]
    heads_here = query_sum.shape[1] // KEY_CHANNELS
    queries = (decay_factor * query_sum).reshape(
        row_count, heads_here, KEY_CHANNELS
    ) * KEY_CHANNELS ** (-0.5)
    key_rows = (decay_factor * key_sum).reshape(row_count, heads_here, KEY_CHANNELS)
    value_rows = (decay_factor * value_sum).reshape(row_count, heads_here, VALUE_DIM)
    gate_rows = (decay_factor * gate_sum).reshape(row_count, heads_here, VALUE_DIM)
    decay_logarithm = (
        jax.nn.log_sigmoid(decay_factor * decay_total) / 16.0 + extra_log_decay
    ).reshape(row_count, heads_here, KEY_CHANNELS)
    new_state = (
        jnp.exp(decay_logarithm)[..., None] * incoming_state
        + key_rows[..., None] * value_rows[:, :, None, :]
    )
    read_out = jnp.einsum("bhk,bhkv->bhv", queries, new_state, precision=lax.Precision.HIGHEST)
    normed = read_out * lax.rsqrt(jnp.mean(read_out * read_out, axis=-1, keepdims=True) + epsilon)
    head_rows = (
        (normed * head_norm_gain * jax.nn.silu(gate_rows))
        .astype(jnp.bfloat16)
        .reshape(row_count, heads_here * VALUE_DIM)
    )
    all_heads = lax.all_gather(head_rows, "kv", axis=0, tiled=True)
    mixed_rows = lax.psum_scatter(
        jnp.dot(all_heads, output_projector, preferred_element_type=jnp.float32),
        ("dp", "tp"),
        scatter_dimension=0,
        tiled=True,
    )
    second = (after_first.astype(jnp.float32) + mixed_rows).astype(jnp.bfloat16)
    result = (
        second.astype(jnp.float32)
        + 0.5
        * channel_mixer(
            second,
            trailing_norm_gain,
            trailing_gate_weight,
            trailing_up_weight,
            trailing_down_weight,
        )
    ).astype(jnp.bfloat16)
    return (result, new_state)


def solution(mesh):
    return jax.shard_map(
        per_device,
        mesh=mesh,
        in_specs=(
            P(("grp", "dp", "tp"), "kv"),
            P(("grp", "kv"), ("dp", "tp"), None, None),
            P(("grp", "kv"), ("dp", "tp")),
            P("kv"),
            P("kv", ("dp", "tp")),
            P("kv", ("dp", "tp")),
            P(("dp", "tp"), "kv"),
            P("kv"),
            P("kv", ("dp", "tp")),
            P("kv", ("dp", "tp")),
            P("kv", ("dp", "tp")),
            P("kv", ("dp", "tp")),
            P("kv", ("dp", "tp")),
            P(),
            P(("dp", "tp"), "kv"),
            P("kv"),
            P("kv", ("dp", "tp")),
            P("kv", ("dp", "tp")),
            P(("dp", "tp"), "kv"),
        ),
        out_specs=(P(("grp", "dp", "tp"), "kv"), P(("grp", "kv"), ("dp", "tp"), None, None)),
        check_vma=False,
    )
```

profile of v0, /device:TPU:0, one launch (start us, length us, event | category | flops | bytes accessed | tf_op | source)
XLA Modules:
  0.0 359.7 jit_solution(16201497556303995588)
XLA Ops:
  7.2 6.9 %all_gather.18 = bf16[64,1024]{1,0:T(8,128)(2,1)S(1)} all-gather(bf16[16,1024]{1,0:T(8,128)(2,1)} %param.19), channel_id=1, replica_groups=mesh['grp'=2,'dp'=2,'kv'=4,'tp'=2] {'dp','tp'}, dimensions={0}, use_global_device_ids=true | all-gather | bytes 163840 | tf_op jit(solution)/shard_map/all_gather | solution.py:13
  14.1 4.6 %fusion.10 = f32[64,2816]{1,0:T(8,128)} fusion(bf16[1024,2816]{1,0:T(8,128)(2,1)} %param.24, bf16[64,1024]{1,0:T(8,128)(2,1)S(1)} %all_gather.18, f32[1024]{0:T(1024)} %param.22), kind=kOutput, calls=%fused_computation.17 | convolution fusion | flops 369295360 | bytes 6623232 | tf_op jit(solution)/shard_map/dot_general | solution.py:22
  18.8 4.6 %fusion.12 = f32[64,2816]{1,0:T(8,128)} fusion(bf16[1024,2816]{1,0:T(8,128)(2,1)} %param.23, bf16[64,1024]{1,0:T(8,128)(2,1)S(1)} %all_gather.18, f32[1024]{0:T(1024)S(1)} %copy-done.7), kind=kOutput, calls=%fused_computation.18 | convolution fusion | flops 369295360 | bytes 6623232 | tf_op jit(solution)/shard_map/dot_general | solution.py:21
  24.9 12.7 %all-reduce = f32[64]{0:T(128)S(1)} all-reduce(f32[64]{0:T(128)S(1)} %fusion), channel_id=2, replica_groups=mesh['grp'=2,'dp'=2,'kv'=4,'tp'=2] {'kv'}, use_global_device_ids=true, to_apply=%region_1.0.clone | all-reduce | flops 64 | bytes 512
  37.6 6.1 %reduce-scatter.15.cloned.1.call-done = f32[16,2816]{1,0:T(8,128)} async-done(((f32[64,2816]{1,0:T(8,128)}), f32[16,2816]{1,0:T(8,128)}) %reduce-scatter.15.cloned.1.call-update) | async-done | bytes 180240 | tf_op jit(solution)/shard_map/reduce_scatter | solution.py:25
  43.7 24.4 %reduce-scatter.13.cloned.1.call-done = f32[16,2816]{1,0:T(8,128)} async-done(((f32[64,2816]{1,0:T(8,128)}), f32[16,2816]{1,0:T(8,128)}) %reduce-scatter.13.cloned.1.call-update) | async-done | bytes 180240 | tf_op jit(solution)/shard_map/reduce_scatter | solution.py:24
  69.3 15.1 %all_gather.19 = bf16[64,2816]{1,0:T(8,128)(2,1)S(1)} all-gather(bf16[16,2816]{1,0:T(8,128)(2,1)S(1)} %multiply_convert_fusion.1), channel_id=1, replica_groups=mesh['grp'=2,'dp'=2,'kv'=4,'tp'=2] {'kv'}, dimensions={0}, use_global_device_ids=true | all-gather | bytes 450560 | tf_op jit(solution)/shard_map/all_gather | solution.py:32
  88.9 19.0 %reduce-scatter.17.cloned.1.call-done = f32[16,1024]{1,0:T(8,128)} async-done(((f32[64,1024]{1,0:T(8,128)}), f32[16,1024]{1,0:T(8,128)}) %reduce-scatter.17.cloned.1.call-update) | async-done | bytes 65552 | tf_op jit(solution)/shard_map/reduce_scatter | solution.py:33
  108.8 5.4 %all_gather.20 = bf16[64,1024]{1,0:T(8,128)(2,1)S(1)} all-gather(bf16[16,1024]{1,0:T(8,128)(2,1)S(1)} %add_convert_fusion.2), channel_id=1, replica_groups=mesh['grp'=2,'dp'=2,'kv'=4,'tp'=2] {'dp','tp'}, dimensions={0}, use_global_device_ids=true | all-gather | bytes 163840 | tf_op jit(solution)/shard_map/all_gather | solution.py:13
  121.3 11.8 %all-reduce.1 = f32[64]{0:T(128)S(1)} all-reduce(f32[64]{0:T(128)S(1)} %fusion.2), channel_id=6, replica_groups=mesh['grp'=2,'dp'=2,'kv'=4,'tp'=2] {'kv'}, use_global_device_ids=true, to_apply=%region_6.7.clone | all-reduce | flops 64 | bytes 512
  135.6 19.5 %reduce-scatter.23.cloned.1.call-done = f32[16,256]{1,0:T(8,128)} async-done(((f32[64,256]{1,0:T(8,128)}), f32[16,256]{1,0:T(8,128)}) %reduce-scatter.23.cloned.1.call-update) | async-done | bytes 16400 | tf_op jit(solution)/shard_map/reduce_scatter | solution.py:84
  155.2 19.6 %reduce-scatter.19.cloned.1.call-done = f32[16,256]{1,0:T(8,128)} async-done(((f32[64,256]{1,0:T(8,128)}), f32[16,256]{1,0:T(8,128)}) %reduce-scatter.19.cloned.1.call-update) | async-done | bytes 16400 | tf_op jit(solution)/shard_map/reduce_scatter | solution.py:83
  175.9 18.8 %reduce-scatter.27.cloned.1.call-done = f32[16,512]{1,0:T(8,128)} async-done(((f32[64,512]{1,0:T(8,128)}), f32[16,512]{1,0:T(8,128)}) %reduce-scatter.27.cloned.1.call-update) | async-done | bytes 32784 | tf_op jit(solution)/shard_map/reduce_scatter | solution.py:86
  194.7 20.5 %reduce-scatter.25.cloned.1.call-done = f32[16,512]{1,0:T(8,128)} async-done(((f32[64,512]{1,0:T(8,128)}), f32[16,512]{1,0:T(8,128)}) %reduce-scatter.25.cloned.1.call-update) | async-done | bytes 32784 | tf_op jit(solution)/shard_map/reduce_scatter | solution.py:85
  220.6 13.1 %all_gather.21 = bf16[64,512]{1,0:T(8,128)(2,1)S(1)} all-gather(bf16[16,512]{1,0:T(8,128)(2,1)S(1)} %bitcast.28), channel_id=1, replica_groups=mesh['grp'=2,'dp'=2,'kv'=4,'tp'=2] {'kv'}, dimensions={0}, use_global_device_ids=true | all-gather | bytes 81920 | tf_op jit(solution)/shard_map/all_gather | solution.py:113
  234.8 18.3 %reduce-scatter.29.cloned.1.call-done = f32[16,1024]{1,0:T(8,128)} async-done(((f32[64,1024]{1,0:T(8,128)}), f32[16,1024]{1,0:T(8,128)}) %reduce-scatter.29.cloned.1.call-update) | async-done | bytes 65552 | tf_op jit(solution)/shard_map/reduce_scatter | solution.py:114
  254.0 5.4 %all_gather.22 = bf16[64,1024]{1,0:T(8,128)(2,1)S(1)} all-gather(bf16[16,1024]{1,0:T(8,128)(2,1)S(1)} %add_convert_fusion.1), channel_id=1, replica_groups=mesh['grp'=2,'dp'=2,'kv'=4,'tp'=2] {'dp','tp'}, dimensions={0}, use_global_device_ids=true | all-gather | bytes 163840 | tf_op jit(solution)/shard_map/all_gather | solution.py:13
  259.4 4.6 %fusion.6 = f32[64,2816]{1,0:T(8,128)} fusion(bf16[1024,2816]{1,0:T(8,128)(2,1)} %param.36, bf16[64,1024]{1,0:T(8,128)(2,1)S(1)} %all_gather.22, f32[1024]{0:T(1024)S(1)} %copy-done.8), kind=kOutput, calls=%fused_computation.15 | convolution fusion | flops 369295360 | bytes 6623232 | tf_op jit(solution)/shard_map/dot_general | solution.py:22
  264.1 4.6 %fusion.8 = f32[64,2816]{1,0:T(8,128)} fusion(bf16[1024,2816]{1,0:T(8,128)(2,1)} %param.35, bf16[64,1024]{1,0:T(8,128)(2,1)S(1)} %all_gather.22, f32[1024]{0:T(1024)S(1)} %copy-done.8), kind=kOutput, calls=%fused_computation.16 | convolution fusion | flops 369295360 | bytes 6623232 | tf_op jit(solution)/shard_map/dot_general | solution.py:21
  268.9 12.0 %all-reduce.2 = f32[64]{0:T(128)S(1)} all-reduce(f32[64]{0:T(128)S(1)} %fusion.4), channel_id=13, replica_groups=mesh['grp'=2,'dp'=2,'kv'=4,'tp'=2] {'kv'}, use_global_device_ids=true, to_apply=%region_15.16.clone | all-reduce | flops 64 | bytes 512
  281.0 6.4 %reduce-scatter.33.cloned.1.call-done = f32[16,2816]{1,0:T(8,128)} async-done(((f32[64,2816]{1,0:T(8,128)}), f32[16,2816]{1,0:T(8,128)}) %reduce-scatter.33.cloned.1.call-update) | async-done | bytes 180240 | tf_op jit(solution)/shard_map/reduce_scatter | solution.py:25
  287.4 24.3 %reduce-scatter.31.cloned.1.call-done = f32[16,2816]{1,0:T(8,128)} async-done(((f32[64,2816]{1,0:T(8,128)}), f32[16,2816]{1,0:T(8,128)}) %reduce-scatter.31.cloned.1.call-update) | async-done | bytes 180240 | tf_op jit(solution)/shard_map/reduce_scatter | solution.py:24
  312.8 14.9 %all_gather.23 = bf16[64,2816]{1,0:T(8,128)(2,1)S(1)} all-gather(bf16[16,2816]{1,0:T(8,128)(2,1)S(1)} %multiply_convert_fusion), channel_id=1, replica_groups=mesh['grp'=2,'dp'=2,'kv'=4,'tp'=2] {'kv'}, dimensions={0}, use_global_device_ids=true | all-gather | bytes 450560 | tf_op jit(solution)/shard_map/all_gather | solution.py:32
  332.2 19.2 %reduce-scatter.35.cloned.1.call-done = f32[16,1024]{1,0:T(8,128)} async-done(((f32[64,1024]{1,0:T(8,128)}), f32[16,1024]{1,0:T(8,128)}) %reduce-scatter.35.cloned.1.call-update) | async-done | bytes 65552 | tf_op jit(solution)/shard_map/reduce_scatter | solution.py:33
  (80 shorter events, 32.8 us)
Async XLA Ops:
  7.2 226.6 %copy-start = (bf16[512,1024]{1,0:T(8,128)(2,1)S(1)}, bf16[512,1024]{1,0:T(8,128)(2,1)}, u32[]{:S(2)}) copy-start(bf16[512,1024]{1,0:T(8,128)(2,1)} %param.33) | copy-start | bytes 3145732
  7.2 11.6 %copy-start.7 = (f32[1024]{0:T(1024)S(1)}, f32[1024]{0:T(1024)}, u32[]{:S(2)}) copy-start(f32[1024]{0:T(1024)} %param.22) | copy-start | bytes 12292
  7.2 36.5 %reduce-scatter.15.cloned.1.call-start = ((), (), s32[]{:S(2)}) async-start(), calls=%async_computation.13 | async-start | bytes 901120 | tf_op jit(solution)/shard_map/reduce_scatter | solution.py:25
  14.1 9.4 %copy-start.10 = (u32[32]{0:T(128)S(1)}, u32[32]{0:T(128)}, u32[]{:S(2)}) copy-start(u32[32]{0:T(128)} %constant.31) | copy-start | bytes 388
  18.8 49.4 %reduce-scatter.13.cloned.1.call-start = ((), (), s32[]{:S(2)}) async-start(), calls=%async_computation.12 | async-start | bytes 901120 | tf_op jit(solution)/shard_map/reduce_scatter | solution.py:24
  23.4 84.5 %copy-start.4 = (bf16[16,1024]{1,0:T(8,128)(2,1)S(1)}, bf16[16,1024]{1,0:T(8,128)(2,1)}, u32[]{:S(2)}) copy-start(bf16[16,1024]{1,0:T(8,128)(2,1)} %param.19) | copy-start | bytes 98308
  23.4 90.8 %copy-start.5 = (f32[1024]{0:T(1024)S(1)}, f32[1024]{0:T(1024)}, u32[]{:S(2)}) copy-start(f32[1024]{0:T(1024)} %param.26) | copy-start | bytes 12292
  23.4 96.7 %copy-start.2 = (bf16[1024,512]{1,0:T(8,128)(2,1)S(1)}, bf16[1024,512]{1,0:T(8,128)(2,1)}, u32[]{:S(2)}) copy-start(bf16[1024,512]{1,0:T(8,128)(2,1)} %param.30) | copy-start | bytes 3145732
  23.5 84.5 %reduce-scatter.17.cloned.1.call-start = ((), (), s32[]{:S(2)}) async-start(), calls=%async_computation.14 | async-start | bytes 327680 | tf_op jit(solution)/shard_map/reduce_scatter | solution.py:33
  69.3 63.8 %copy-start.3 = (bf16[1024,512]{1,0:T(8,128)(2,1)S(1)}, bf16[1024,512]{1,0:T(8,128)(2,1)}, u32[]{:S(2)}) copy-start(bf16[1024,512]{1,0:T(8,128)(2,1)} %param.29) | copy-start | bytes 3145732
  84.4 90.4 %copy-start.6 = (f32[16,256]{1,0:T(8,128)S(1)}, f32[16,256]{1,0:T(8,128)}, u32[]{:S(2)}) copy-start(f32[16,256]{1,0:T(8,128)} %param.21) | copy-start | bytes 49156
  88.9 46.8 %reduce-scatter.21.cloned.1.call-start = ((), (), s32[]{:S(2)}) async-start(), calls=%async_computation.16 | async-start | bytes 81920 | tf_op jit(solution)/shard_map/reduce_scatter | solution.py:87
  116.2 104.3 %copy-start.9 = (f32[128]{0:T(128)S(1)}, f32[128]{0:T(128)}, u32[]{:S(2)}) copy-start(f32[128]{0:T(128)} %param.32) | copy-start | bytes 1540
  116.2 39.0 %reduce-scatter.23.cloned.1.call-start = ((), (), s32[]{:S(2)}) async-start(), calls=%async_computation.17 | async-start | bytes 81920 | tf_op jit(solution)/shard_map/reduce_scatter | solution.py:84
  118.1 56.6 %reduce-scatter.19.cloned.1.call-start = ((), (), s32[]{:S(2)}) async-start(), calls=%async_computation.15 | async-start | bytes 81920 | tf_op jit(solution)/shard_map/reduce_scatter | solution.py:83
  120.1 74.6 %reduce-scatter.27.cloned.1.call-start = ((), (), s32[]{:S(2)}) async-start(), calls=%async_computation.19 | async-start | bytes 163840 | tf_op jit(solution)/shard_map/reduce_scatter | solution.py:86
  121.1 138.3 %copy-start.8 = (f32[1024]{0:T(1024)S(1)}, f32[1024]{0:T(1024)}, u32[]{:S(2)}) copy-start(f32[1024]{0:T(1024)} %param.34) | copy-start | bytes 12292
  121.1 94.1 %reduce-scatter.25.cloned.1.call-start = ((), (), s32[]{:S(2)}) async-start(), calls=%async_computation.18 | async-start | bytes 163840 | tf_op jit(solution)/shard_map/reduce_scatter | solution.py:85
  134.0 119.1 %reduce-scatter.29.cloned.1.call-start = ((), (), s32[]{:S(2)}) async-start(), calls=%async_computation.20 | async-start | bytes 327680 | tf_op jit(solution)/shard_map/reduce_scatter | solution.py:114
  218.5 45.5 %copy-start.1 = (f32[16,4,64,128]{3,2,1,0:T(8,128)}, f32[16,4,64,128]{3,2,1,0:T(8,128)S(1)}, u32[]{:S(2)}) copy-start(f32[16,4,64,128]{3,2,1,0:T(8,128)S(1)} %multiply_add_fusion) | copy-start | bytes 6291460
  234.7 52.6 %reduce-scatter.33.cloned.1.call-start = ((), (), s32[]{:S(2)}) async-start(), calls=%async_computation.22 | async-start | bytes 901120 | tf_op jit(solution)/shard_map/reduce_scatter | solution.py:25
  264.0 47.6 %reduce-scatter.31.cloned.1.call-start = ((), (), s32[]{:S(2)}) async-start(), calls=%async_computation.21 | async-start | bytes 901120 | tf_op jit(solution)/shard_map/reduce_scatter | solution.py:24
  268.7 82.7 %reduce-scatter.35.cloned.1.call-start = ((), (), s32[]{:S(2)}) async-start(), calls=%async_computation.23 | async-start | bytes 327680 | tf_op jit(solution)/shard_map/reduce_scatter | solution.py:33
Sparse Core Ops, SparseCore 0:
  18.9 24.7 reduce-scatter.14
  46.0 22.0 reduce-scatter.12
  89.0 18.9 reduce-scatter.16
  116.3 19.3 reduce-scatter.20
  137.7 17.4 reduce-scatter.22
  157.3 17.4 reduce-scatter.18
  177.0 17.6 reduce-scatter.26
  197.5 17.6 reduce-scatter.24
  234.9 18.2 reduce-scatter.28
  264.1 23.1 reduce-scatter.32
  289.7 21.9 reduce-scatter.30
  332.3 18.9 reduce-scatter.34
where the time goes:
time: 361 us; the launch traced here: 360 us
  waiting for transfers between devices  198 us (55%)
  blocking collectives  97.3 us (27%)
  matrix products  37.8 us (10%)
  between operations  15 us (4%)
  other arithmetic  10.4 us (3%)
    reduce_scatter x2, waiting for transfers between devices, channel_mixer(): lax.psum_scatter(gate_part, 'kv', scatter_dimension=0, tiled=True)  48.7 us
    reduce_scatter x2, waiting for transfers between devices, channel_mixer(): lax.psum_scatter(jnp.dot(hidden, down_matrix, preferred_element_type=jnp....  38.2 us
    unnamed x3, blocking collectives  36.4 us
    all_gather x2, blocking collectives, channel_mixer(): hidden = lax.all_gather(hidden_share, 'kv', axis=0, tiled=True)  30 us
    reduce_scatter x1, waiting for transfers between devices, per_device(): lax.psum_scatter(value_part, 'kv', scatter_dimension=0, tiled=True)  20.5 us
    reduce_scatter x1, waiting for transfers between devices, per_device(): lax.psum_scatter(query_part, 'kv', scatter_dimension=0, tiled=True)  19.6 us
    reduce_scatter x1, waiting for transfers between devices, per_device(): lax.psum_scatter(key_part, 'kv', scatter_dimension=0, tiled=True)  19.5 us
    reduce_scatter x1, waiting for transfers between devices, per_device(): lax.psum_scatter(gate_part, 'kv', scatter_dimension=0, tiled=True)  18.8 us
  transfers between devices with their start and end apart: 12, of which 12 were waited for; matrix products, arithmetic and copies ran while one was open for 5% of the time, Pallas kernels for 0%

commit v1 on v0

--- a/solution.py
+++ b/solution.py
@@ -29,7 +29,14 @@
     hidden_share = (jax.nn.silu(decay_factor * gate_sum) * (decay_factor * up_sum)).astype(
         jnp.bfloat16
     )
-    hidden = lax.all_gather(hidden_share, "kv", axis=0, tiled=True)
+    size = lax.axis_size("kv")
+    right = [(i, (i + 1) % size) for i in range(size)]
+    parts = [hidden_share]
+    for hop in range(1, size):
+        parts = [lax.ppermute(parts[0], "kv", right), *parts]
+    whole = jnp.concatenate(parts, axis=0)
+    shift = (lax.axis_index("kv") + 1) * parts[-1].shape[0]
+    hidden = jnp.roll(whole, shift, axis=0)
     return lax.psum_scatter(
         jnp.dot(hidden, down_matrix, preferred_element_type=jnp.float32),
         ("dp", "tp"),

time: 361 us -> 369 us (1.022)
  waiting for transfers between devices: 198 us -> 235 us
  blocking collectives: 97.3 us -> 67.3 us
    ppermute x0 -> x6, waiting for transfers between devices: none -> 38.9 us  [channel_mixer(): parts = [lax.ppermute(parts[0], 'kv', right), *parts]]
    all_gather x2 -> x0, blocking collectives: 30 us -> none  [channel_mixer(): hidden = lax.all_gather(hidden_share, 'kv', axis=0, tiled=True)]
  transfers between devices with their start and end apart: 12 -> 18, of which waited for: 12 -> 18; matrix products, arithmetic and copies ran while one was open for 5% -> 5% of each run, Pallas kernels for 0% -> 0%
where the time goes in v1:
time: 369 us; the launch traced here: 368 us
  waiting for transfers between devices  235 us (64%)
  blocking collectives  67.3 us (18%)
  matrix products  38.6 us (10%)
  between operations  15 us (4%)
  other arithmetic  10.4 us (3%)
    reduce_scatter x2, waiting for transfers between devices, channel_mixer(): lax.psum_scatter(gate_part, 'kv', scatter_dimension=0, tiled=True)  48.8 us
    ppermute x6, waiting for transfers between devices, channel_mixer(): parts = [lax.ppermute(parts[0], 'kv', right), *parts]  38.9 us
    reduce_scatter x2, waiting for transfers between devices, channel_mixer(): lax.psum_scatter(jnp.dot(hidden, down_matrix, preferred_element_type=jnp....  36.6 us
    unnamed x3, blocking collectives  36.4 us
    reduce_scatter x1, waiting for transfers between devices, per_device(): lax.psum_scatter(value_part, 'kv', scatter_dimension=0, tiled=True)  20.4 us
    reduce_scatter x1, waiting for transfers between devices, per_device(): lax.psum_scatter(key_part, 'kv', scatter_dimension=0, tiled=True)  19.6 us
    reduce_scatter x1, waiting for transfers between devices, per_device(): lax.psum_scatter(query_part, 'kv', scatter_dimension=0, tiled=True)  19.6 us
    reduce_scatter x1, waiting for transfers between devices, per_device(): lax.psum_scatter(gate_part, 'kv', scatter_dimension=0, tiled=True)  18.8 us
  transfers between devices with their start and end apart: 18, of which 18 were waited for; matrix products, arithmetic and copies ran while one was open for 5% of the time, Pallas kernels for 0%

profile of v1, /device:TPU:0, one launch (start us, length us, event | category | flops | bytes accessed | tf_op | source)
XLA Modules:
  0.0 368.0 jit_solution(7678598062760464416)
XLA Ops:
  7.2 6.9 %all_gather.12 = bf16[64,1024]{1,0:T(8,128)(2,1)S(1)} all-gather(bf16[16,1024]{1,0:T(8,128)(2,1)} %param.21), channel_id=1, replica_groups=mesh['grp'=2,'dp'=2,'kv'=4,'tp'=2] {'dp','tp'}, dimensions={0}, use_global_device_ids=true | all-gather | bytes 163840 | tf_op jit(solution)/shard_map/all_gather | solution.py:13
  24.9 12.7 %all-reduce = f32[64]{0:T(128)S(1)} all-reduce(f32[64]{0:T(128)S(1)} %fusion.20), channel_id=2, replica_groups=mesh['grp'=2,'dp'=2,'kv'=4,'tp'=2] {'kv'}, use_global_device_ids=true, to_apply=%region_1.0.clone | all-reduce | flops 64 | bytes 512
  37.7 6.0 %reduce-scatter.15.cloned.1.call-done = f32[16,2816]{1,0:T(8,128)} async-done(((f32[64,2816]{1,0:T(8,128)}), f32[16,2816]{1,0:T(8,128)}) %reduce-scatter.15.cloned.1.call-update) | async-done | bytes 180240 | tf_op jit(solution)/shard_map/reduce_scatter | solution.py:25
  43.7 24.4 %reduce-scatter.13.cloned.1.call-done = f32[16,2816]{1,0:T(8,128)} async-done(((f32[64,2816]{1,0:T(8,128)}), f32[16,2816]{1,0:T(8,128)}) %reduce-scatter.13.cloned.1.call-update) | async-done | bytes 180240 | tf_op jit(solution)/shard_map/reduce_scatter | solution.py:24
  69.3 6.3 %collective-permute-done = bf16[16,2816]{1,0:T(8,128)(2,1)S(1)} collective-permute-done((bf16[16,2816]{1,0:T(8,128)(2,1)S(1)}, bf16[16,2816]{1,0:T(8,128)(2,1)S(1)}, u32[]{:S(2)}, u32[]{:S(2)}) %collective-permute-start) | collective-permute-done | bytes 90144 | tf_op jit(solution)/shard_map/ppermute | solution.py:36
  75.6 6.7 %collective-permute-done.1 = bf16[16,2816]{1,0:T(8,128)(2,1)S(1)} collective-permute-done((bf16[16,2816]{1,0:T(8,128)(2,1)S(1)}, bf16[16,2816]{1,0:T(8,128)(2,1)S(1)}, u32[]{:S(2)}, u32[]{:S(2)}) %collective-permute-start.1) | collective-permute-done | bytes 90144 | tf_op jit(solution)/shard_map/ppermute | solution.py:36
  82.4 6.4 %collective-permute-done.2 = bf16[16,2816]{1,0:T(8,128)(2,1)} collective-permute-done((bf16[16,2816]{1,0:T(8,128)(2,1)S(1)}, bf16[16,2816]{1,0:T(8,128)(2,1)}, u32[]{:S(2)}, u32[]{:S(2)}) %collective-permute-start.2) | collective-permute-done | bytes 90144 | tf_op jit(solution)/shard_map/ppermute | solution.py:36
  93.8 18.2 %reduce-scatter.17.cloned.1.call-done = f32[16,1024]{1,0:T(8,128)} async-done(((f32[64,1024]{1,0:T(8,128)}), f32[16,1024]{1,0:T(8,128)}) %reduce-scatter.17.cloned.1.call-update) | async-done | bytes 65552 | tf_op jit(solution)/shard_map/reduce_scatter | solution.py:40
  112.8 5.4 %all_gather.13 = bf16[64,1024]{1,0:T(8,128)(2,1)S(1)} all-gather(bf16[16,1024]{1,0:T(8,128)(2,1)S(1)} %add_convert_fusion.2), channel_id=1, replica_groups=mesh['grp'=2,'dp'=2,'kv'=4,'tp'=2] {'dp','tp'}, dimensions={0}, use_global_device_ids=true | all-gather | bytes 163840 | tf_op jit(solution)/shard_map/all_gather | solution.py:13
  125.3 11.7 %all-reduce.1 = f32[64]{0:T(128)S(1)} all-reduce(f32[64]{0:T(128)S(1)} %fusion.22), channel_id=6, replica_groups=mesh['grp'=2,'dp'=2,'kv'=4,'tp'=2] {'kv'}, use_global_device_ids=true, to_apply=%region_6.8.clone | all-reduce | flops 64 | bytes 512
  139.6 19.6 %reduce-scatter.23.cloned.1.call-done = f32[16,256]{1,0:T(8,128)} async-done(((f32[64,256]{1,0:T(8,128)}), f32[16,256]{1,0:T(8,128)}) %reduce-scatter.23.cloned.1.call-update) | async-done | bytes 16400 | tf_op jit(solution)/shard_map/reduce_scatter | solution.py:91
  159.2 19.6 %reduce-scatter.19.cloned.1.call-done = f32[16,256]{1,0:T(8,128)} async-done(((f32[64,256]{1,0:T(8,128)}), f32[16,256]{1,0:T(8,128)}) %reduce-scatter.19.cloned.1.call-update) | async-done | bytes 16400 | tf_op jit(solution)/shard_map/reduce_scatter | solution.py:90
  179.9 18.8 %reduce-scatter.27.cloned.1.call-done = f32[16,512]{1,0:T(8,128)} async-done(((f32[64,512]{1,0:T(8,128)}), f32[16,512]{1,0:T(8,128)}) %reduce-scatter.27.cloned.1.call-update) | async-done | bytes 32784 | tf_op jit(solution)/shard_map/reduce_scatter | solution.py:93
  198.7 20.4 %reduce-scatter.25.cloned.1.call-done = f32[16,512]{1,0:T(8,128)} async-done(((f32[64,512]{1,0:T(8,128)}), f32[16,512]{1,0:T(8,128)}) %reduce-scatter.25.cloned.1.call-update) | async-done | bytes 32784 | tf_op jit(solution)/shard_map/reduce_scatter | solution.py:92
  224.6 13.1 %all_gather.14 = bf16[64,512]{1,0:T(8,128)(2,1)S(1)} all-gather(bf16[16,512]{1,0:T(8,128)(2,1)S(1)} %bitcast.26), channel_id=1, replica_groups=mesh['grp'=2,'dp'=2,'kv'=4,'tp'=2] {'kv'}, dimensions={0}, use_global_device_ids=true | all-gather | bytes 81920 | tf_op jit(solution)/shard_map/all_gather | solution.py:120
  238.8 18.4 %reduce-scatter.29.cloned.1.call-done = f32[16,1024]{1,0:T(8,128)} async-done(((f32[64,1024]{1,0:T(8,128)}), f32[16,1024]{1,0:T(8,128)}) %reduce-scatter.29.cloned.1.call-update) | async-done | bytes 65552 | tf_op jit(solution)/shard_map/reduce_scatter | solution.py:121
  258.0 5.4 %all_gather.15 = bf16[64,1024]{1,0:T(8,128)(2,1)S(1)} all-gather(bf16[16,1024]{1,0:T(8,128)(2,1)S(1)} %add_convert_fusion.1), channel_id=1, replica_groups=mesh['grp'=2,'dp'=2,'kv'=4,'tp'=2] {'dp','tp'}, dimensions={0}, use_global_device_ids=true | all-gather | bytes 163840 | tf_op jit(solution)/shard_map/all_gather | solution.py:13
  273.0 12.0 %all-reduce.2 = f32[64]{0:T(128)S(1)} all-reduce(f32[64]{0:T(128)S(1)} %fusion.24), channel_id=13, replica_groups=mesh['grp'=2,'dp'=2,'kv'=4,'tp'=2] {'kv'}, use_global_device_ids=true, to_apply=%region_15.17.clone | all-reduce | flops 64 | bytes 512
  285.1 6.3 %reduce-scatter.33.cloned.1.call-done = f32[16,2816]{1,0:T(8,128)} async-done(((f32[64,2816]{1,0:T(8,128)}), f32[16,2816]{1,0:T(8,128)}) %reduce-scatter.33.cloned.1.call-update) | async-done | bytes 180240 | tf_op jit(solution)/shard_map/reduce_scatter | solution.py:25
  291.4 24.3 %reduce-scatter.31.cloned.1.call-done = f32[16,2816]{1,0:T(8,128)} async-done(((f32[64,2816]{1,0:T(8,128)}), f32[16,2816]{1,0:T(8,128)}) %reduce-scatter.31.cloned.1.call-update) | async-done | bytes 180240 | tf_op jit(solution)/shard_map/reduce_scatter | solution.py:24
  316.9 6.3 %collective-permute-done.3 = bf16[16,2816]{1,0:T(8,128)(2,1)S(1)} collective-permute-done((bf16[16,2816]{1,0:T(8,128)(2,1)S(1)}, bf16[16,2816]{1,0:T(8,128)(2,1)S(1)}, u32[]{:S(2)}, u32[]{:S(2)}) %collective-permute-start.3) | collective-permute-done | bytes 90144 | tf_op jit(solution)/shard_map/ppermute | solution.py:36
  323.2 6.7 %collective-permute-done.4 = bf16[16,2816]{1,0:T(8,128)(2,1)S(1)} collective-permute-done((bf16[16,2816]{1,0:T(8,128)(2,1)S(1)}, bf16[16,2816]{1,0:T(8,128)(2,1)S(1)}, u32[]{:S(2)}, u32[]{:S(2)}) %collective-permute-start.4) | collective-permute-done | bytes 90144 | tf_op jit(solution)/shard_map/ppermute | solution.py:36
  330.0 6.3 %collective-permute-done.5 = bf16[16,2816]{1,0:T(8,128)(2,1)S(1)} collective-permute-done((bf16[16,2816]{1,0:T(8,128)(2,1)S(1)}, bf16[16,2816]{1,0:T(8,128)(2,1)S(1)}, u32[]{:S(2)}, u32[]{:S(2)}) %collective-permute-start.5) | collective-permute-done | bytes 90144 | tf_op jit(solution)/shard_map/ppermute | solution.py:36
  341.2 18.4 %reduce-scatter.35.cloned.1.call-done = f32[16,1024]{1,0:T(8,128)} async-done(((f32[64,1024]{1,0:T(8,128)}), f32[16,1024]{1,0:T(8,128)}) %reduce-scatter.35.cloned.1.call-update) | async-done | bytes 65552 | tf_op jit(solution)/shard_map/reduce_scatter | solution.py:40
  (90 shorter events, 52.3 us)
Async XLA Ops:
  7.2 230.6 %copy-start = (bf16[512,1024]{1,0:T(8,128)(2,1)S(1)}, bf16[512,1024]{1,0:T(8,128)(2,1)}, u32[]{:S(2)}) copy-start(bf16[512,1024]{1,0:T(8,128)(2,1)} %param.35) | copy-start | bytes 3145732
  7.2 36.5 %reduce-scatter.15.cloned.1.call-start = ((), (), s32[]{:S(2)}) async-start(), calls=%async_computation.13 | async-start | bytes 901120 | tf_op jit(solution)/shard_map/reduce_scatter | solution.py:25
  18.8 49.4 %reduce-scatter.13.cloned.1.call-start = ((), (), s32[]{:S(2)}) async-start(), calls=%async_computation.12 | async-start | bytes 901120 | tf_op jit(solution)/shard_map/reduce_scatter | solution.py:24
  23.4 94.8 %copy-start.5 = (f32[1024]{0:T(1024)S(1)}, f32[1024]{0:T(1024)}, u32[]{:S(2)}) copy-start(f32[1024]{0:T(1024)} %param.28) | copy-start | bytes 12292
  23.5 88.5 %reduce-scatter.17.cloned.1.call-start = ((), (), s32[]{:S(2)}) async-start(), calls=%async_computation.14 | async-start | bytes 327680 | tf_op jit(solution)/shard_map/reduce_scatter | solution.py:40
  24.9 99.2 %copy-start.2 = (bf16[1024,512]{1,0:T(8,128)(2,1)S(1)}, bf16[1024,512]{1,0:T(8,128)(2,1)}, u32[]{:S(2)}) copy-start(bf16[1024,512]{1,0:T(8,128)(2,1)} %param.32) | copy-start | bytes 3145732
  69.3 6.4 %collective-permute-start = (bf16[16,2816]{1,0:T(8,128)(2,1)S(1)}, bf16[16,2816]{1,0:T(8,128)(2,1)S(1)}, u32[]{:S(2)}, u32[]{:S(2)}) collective-permute-start(bf16[16,2816]{1,0:T(8,128)(2,1)S(1)} %multiply_convert_fusion.1), channel_id=1, source_target_pairs={{0,2},{2,4},{4,6},{6,0},{1,3},{3,5},{5,7},{7,1},{8,10},{10,12},{12... | collective-permute-start | bytes 270344 | tf_op jit(solution)/shard_map/ppermute | solution.py:36
  75.6 6.7 %collective-permute-start.1 = (bf16[16,2816]{1,0:T(8,128)(2,1)S(1)}, bf16[16,2816]{1,0:T(8,128)(2,1)S(1)}, u32[]{:S(2)}, u32[]{:S(2)}) collective-permute-start(bf16[16,2816]{1,0:T(8,128)(2,1)S(1)} %collective-permute-done), channel_id=1, source_target_pairs={{0,2},{2,4},{4,6},{6,0},{1,3},{3,5},{5,7},{7,1},{8,10},{10,12},{12... | collective-permute-start | bytes 270344 | tf_op jit(solution)/shard_map/ppermute | solution.py:36
  82.4 6.4 %collective-permute-start.2 = (bf16[16,2816]{1,0:T(8,128)(2,1)S(1)}, bf16[16,2816]{1,0:T(8,128)(2,1)}, u32[]{:S(2)}, u32[]{:S(2)}) collective-permute-start(bf16[16,2816]{1,0:T(8,128)(2,1)S(1)} %collective-permute-done.1), channel_id=1, source_target_pairs={{0,2},{2,4},{4,6},{6,0},{1,3},{3,5},{5,7},{7,1},{8,10},{10,12},{12... | collective-permute-start | bytes 270344 | tf_op jit(solution)/shard_map/ppermute | solution.py:36
  82.4 96.4 %copy-start.6 = (f32[16,256]{1,0:T(8,128)S(1)}, f32[16,256]{1,0:T(8,128)}, u32[]{:S(2)}) copy-start(f32[16,256]{1,0:T(8,128)} %param.23) | copy-start | bytes 49156
  93.7 45.9 %reduce-scatter.21.cloned.1.call-start = ((), (), s32[]{:S(2)}) async-start(), calls=%async_computation.16 | async-start | bytes 81920 | tf_op jit(solution)/shard_map/reduce_scatter | solution.py:94
  120.2 104.4 %copy-start.9 = (f32[128]{0:T(128)S(1)}, f32[128]{0:T(128)}, u32[]{:S(2)}) copy-start(f32[128]{0:T(128)} %param.34) | copy-start | bytes 1540
  120.2 39.0 %reduce-scatter.23.cloned.1.call-start = ((), (), s32[]{:S(2)}) async-start(), calls=%async_computation.17 | async-start | bytes 81920 | tf_op jit(solution)/shard_map/reduce_scatter | solution.py:91
  122.1 56.7 %reduce-scatter.19.cloned.1.call-start = ((), (), s32[]{:S(2)}) async-start(), calls=%async_computation.15 | async-start | bytes 81920 | tf_op jit(solution)/shard_map/reduce_scatter | solution.py:90
  124.1 74.7 %reduce-scatter.27.cloned.1.call-start = ((), (), s32[]{:S(2)}) async-start(), calls=%async_computation.19 | async-start | bytes 163840 | tf_op jit(solution)/shard_map/reduce_scatter | solution.py:93
  125.1 138.4 %copy-start.8 = (f32[1024]{0:T(1024)S(1)}, f32[1024]{0:T(1024)}, u32[]{:S(2)}) copy-start(f32[1024]{0:T(1024)} %param.36) | copy-start | bytes 12292
  125.1 94.1 %reduce-scatter.25.cloned.1.call-start = ((), (), s32[]{:S(2)}) async-start(), calls=%async_computation.18 | async-start | bytes 163840 | tf_op jit(solution)/shard_map/reduce_scatter | solution.py:92
  138.0 119.2 %reduce-scatter.29.cloned.1.call-start = ((), (), s32[]{:S(2)}) async-start(), calls=%async_computation.20 | async-start | bytes 327680 | tf_op jit(solution)/shard_map/reduce_scatter | solution.py:121
  238.8 52.6 %reduce-scatter.33.cloned.1.call-start = ((), (), s32[]{:S(2)}) async-start(), calls=%async_computation.22 | async-start | bytes 901120 | tf_op jit(solution)/shard_map/reduce_scatter | solution.py:25
  268.1 47.6 %reduce-scatter.31.cloned.1.call-start = ((), (), s32[]{:S(2)}) async-start(), calls=%async_computation.21 | async-start | bytes 901120 | tf_op jit(solution)/shard_map/reduce_scatter | solution.py:24
  272.8 86.9 %reduce-scatter.35.cloned.1.call-start = ((), (), s32[]{:S(2)}) async-start(), calls=%async_computation.23 | async-start | bytes 327680 | tf_op jit(solution)/shard_map/reduce_scatter | solution.py:40
  316.9 6.4 %collective-permute-start.3 = (bf16[16,2816]{1,0:T(8,128)(2,1)S(1)}, bf16[16,2816]{1,0:T(8,128)(2,1)S(1)}, u32[]{:S(2)}, u32[]{:S(2)}) collective-permute-start(bf16[16,2816]{1,0:T(8,128)(2,1)S(1)} %multiply_convert_fusion), channel_id=1, source_target_pairs={{0,2},{2,4},{4,6},{6,0},{1,3},{3,5},{5,7},{7,1},{8,10},{10,12},{12... | collective-permute-start | bytes 270344 | tf_op jit(solution)/shard_map/ppermute | solution.py:36
  323.2 6.7 %collective-permute-start.4 = (bf16[16,2816]{1,0:T(8,128)(2,1)S(1)}, bf16[16,2816]{1,0:T(8,128)(2,1)S(1)}, u32[]{:S(2)}, u32[]{:S(2)}) collective-permute-start(bf16[16,2816]{1,0:T(8,128)(2,1)S(1)} %collective-permute-done.3), channel_id=1, source_target_pairs={{0,2},{2,4},{4,6},{6,0},{1,3},{3,5},{5,7},{7,1},{8,10},{10,12},{12... | collective-permute-start | bytes 270344 | tf_op jit(solution)/shard_map/ppermute | solution.py:36
  330.0 6.3 %collective-permute-start.5 = (bf16[16,2816]{1,0:T(8,128)(2,1)S(1)}, bf16[16,2816]{1,0:T(8,128)(2,1)S(1)}, u32[]{:S(2)}, u32[]{:S(2)}) collective-permute-start(bf16[16,2816]{1,0:T(8,128)(2,1)S(1)} %collective-permute-done.4), channel_id=1, source_target_pairs={{0,2},{2,4},{4,6},{6,0},{1,3},{3,5},{5,7},{7,1},{8,10},{10,12},{12... | collective-permute-start | bytes 270344 | tf_op jit(solution)/shard_map/ppermute | solution.py:36
  (5 other events, 209.8 us)
Sparse Core Ops, SparseCore 0:
  18.9 24.7 reduce-scatter.14
  46.0 22.0 reduce-scatter.12
  93.9 18.0 reduce-scatter.16
  120.3 19.2 reduce-scatter.20
  141.7 17.4 reduce-scatter.22
  161.3 17.4 reduce-scatter.18
  181.1 17.6 reduce-scatter.26
  201.5 17.5 reduce-scatter.24
  238.9 18.2 reduce-scatter.28
  268.2 23.1 reduce-scatter.32
  293.7 21.9 reduce-scatter.30
  341.4 18.2 reduce-scatter.34
